TPU v7x, 32 devices: a whole 2x2x4 slice. The times are simulated.
32 devices in a mesh: sp: 8 (over z, x), dp: 4 (over y, core).
Axes of the slice: x: 2, y: 2, z: 4, core: 2. Of those that a mesh axis runs over, the one named last changes fastest.
Arguments:
- hidden_in: bfloat16 [4, 1024, 2048], P('dp', 'sp'), may hold values from -6 to 6
- mix_cotangent: bfloat16 [4, 1024, 4096], P('dp', 'sp'), may hold values from -0.119628906 to 0.119628906
- query_weight: bfloat16 [2048, 4096], P('dp', 'sp'), may hold values from -0.125 to 0.125
- key_weight: bfloat16 [2048, 4096], P('dp', 'sp'), may hold values from -0.125 to 0.125
- value_weight: bfloat16 [2048, 4096], P('dp', 'sp'), may hold values from -0.125 to 0.125
- decay_log: float32 [16], P('sp'), may hold values from -0.034 to -0.00029296875, as said below
Outputs:
- grad_hidden: bfloat16 [4, 1024, 2048], P('dp', 'sp')
- grad_query: float32 [2048, 4096], P('dp', 'sp')
- grad_key: float32 [2048, 4096], P('dp', 'sp')
- grad_value: float32 [2048, 4096], P('dp', 'sp')
Inputs may be any that keep to these rules, and one draw needn't show every extreme that they name: Each head's decay_log is negative.
All inputs are finite; a program needn't handle non-finite values.
Results may differ from a plain program's by a relative error of at most 0.015.
Values may be sent and summed in bfloat16 or wider, within the bound.
A program may use at most 64 MiB of HBM per device.

v0:
```python
import jax
import jax.numpy as jnp
from jax import lax
from jax.sharding import PartitionSpec as P

BLOCK = 128


def head_grads(queries, key_rows, values, cotangent, log_rate):
    length = queries.shape[0]
    head_dim = queries.shape[1]
    blocks = length // BLOCK
    scale = head_dim ** (-0.5)
    keys_scaled = (key_rows.astype(jnp.float32) * scale).astype(jnp.bfloat16)
    offsets = jnp.arange(BLOCK, dtype=jnp.float32)
    spread = offsets[:, None] - offsets[None, :]
    inner_decay = jnp.where(spread >= 0, jnp.exp(log_rate * jnp.maximum(spread, 0.0)), 0.0)
    query_decay = jnp.exp(log_rate * (offsets + 1.0))
    key_decay = jnp.exp(log_rate * (BLOCK - 1.0 - offsets))
    block_decay = jnp.exp(log_rate * BLOCK)

    def split_blocks(series):
        return series.reshape(blocks, BLOCK, series.shape[-1])

    def forward(carried, inputs):
        query_block, key_block, value_block, grad_block = inputs
        mixed = (
            jnp.dot(grad_block, value_block.T, preferred_element_type=jnp.float32) * inner_decay
        ).astype(jnp.bfloat16)
        within = jnp.dot(mixed, key_block, preferred_element_type=jnp.float32)
        across = (
            jnp.dot(grad_block, carried.astype(jnp.bfloat16).T, preferred_element_type=jnp.float32)
            * query_decay[:, None]
        )
        weighted = (key_block.astype(jnp.float32) * key_decay[:, None]).astype(jnp.bfloat16)
        updated = carried * block_decay + jnp.dot(
            weighted.T, value_block, preferred_element_type=jnp.float32
        )
        return (updated, (within + across, mixed))

    def backward(carried, inputs):
        query_block, key_block, value_block, grad_block, mixed = inputs
        scores = (
            jnp.dot(query_block, key_block.T, preferred_element_type=jnp.float32) * inner_decay
        ).astype(jnp.bfloat16)
        state_bf = carried.astype(jnp.bfloat16)
        grad_v = (
            jnp.dot(scores.T, grad_block, preferred_element_type=jnp.float32)
            + jnp.dot(key_block, state_bf, preferred_element_type=jnp.float32) * key_decay[:, None]
        )
        grad_k = (
            jnp.dot(mixed.T, query_block, preferred_element_type=jnp.float32)
            + jnp.dot(value_block, state_bf.T, preferred_element_type=jnp.float32)
            * key_decay[:, None]
        ) * scale
        weighted = (query_block.astype(jnp.float32) * query_decay[:, None]).astype(jnp.bfloat16)
        updated = carried * block_decay + jnp.dot(
            weighted.T, grad_block, preferred_element_type=jnp.float32
        )
        return (updated, (grad_k, grad_v))

    inputs = (
        split_blocks(queries),
        split_blocks(keys_scaled),
        split_blocks(values),
        split_blocks(cotangent),
    )
    initial = jnp.zeros((head_dim, values.shape[-1]), jnp.float32)
    final_state, (grad_q, mixed_all) = lax.scan(forward, initial, inputs)
    final_back, (grad_k, grad_v) = lax.scan(backward, initial, inputs + (mixed_all,), reverse=True)
    return (grad_q.reshape(length, -1), grad_k.reshape(length, -1), grad_v.reshape(length, -1))


def group_grads(log_rates, queries, key_rows, values, cotangent):
    length = queries.shape[0]
    head_count = log_rates.shape[0]

    def by_head(series):
        return series.reshape(length, head_count, -1).transpose(1, 0, 2)

    def to_rows(series):
        return series.transpose(1, 0, 2).reshape(length, -1)

    grad_q, grad_k, grad_v = jax.vmap(head_grads)(
        by_head(queries), by_head(key_rows), by_head(values), by_head(cotangent), log_rates
    )
    return jnp.concatenate((to_rows(grad_q), to_rows(grad_k), to_rows(grad_v)), axis=1).astype(
        jnp.bfloat16
    )


def body(hidden_in, mix_cotangent, query_weight, key_weight, value_weight, decay_log):
    own_rows = hidden_in[0]
    columns = query_weight.shape[1]
    stacked = jnp.stack((query_weight, key_weight, value_weight), axis=1)
    gathered = lax.all_gather(stacked, "dp", axis=0, tiled=True)
    weights = gathered.reshape(gathered.shape[0], 3 * columns)
    cotangent = lax.all_to_all(mix_cotangent[0], "sp", split_axis=1, concat_axis=0, tiled=True)
    all_rows = lax.all_gather(own_rows, "sp", axis=0, tiled=True)
    projected = jnp.dot(all_rows, weights, preferred_element_type=jnp.float32).astype(jnp.bfloat16)
    gradients = group_grads(
        decay_log,
        projected[:, :columns],
        projected[:, columns : 2 * columns],
        projected[:, 2 * columns :],
        cotangent,
    )
    input_sum = lax.psum_scatter(
        lax.dot_general(
            gradients, weights, (((1,), (1,)), ((), ())), preferred_element_type=jnp.float32
        ).astype(jnp.bfloat16),
        "sp",
        scatter_dimension=0,
        tiled=True,
    )
    grad_hidden = input_sum[None]
    summed = lax.psum_scatter(
        lax.dot_general(
            all_rows, gradients, (((0,), (0,)), ((), ())), preferred_element_type=jnp.float32
        ).astype(jnp.bfloat16),
        "dp",
        scatter_dimension=0,
        tiled=True,
    ).astype(jnp.float32) / lax.axis_size("dp")
    return (
        grad_hidden,
        summed[:, :columns],
        summed[:, columns : 2 * columns],
        summed[:, 2 * columns :],
    )


def solution(mesh):
    placed = (
        P("dp", "sp", None),
        P("dp", "sp", None),
        P("dp", "sp"),
        P("dp", "sp"),
        P("dp", "sp"),
        P("sp"),
    )
    return jax.shard_map(
        body,
        mesh=mesh,
        in_specs=placed,
        out_specs=(P("dp", "sp", None), P("dp", "sp"), P("dp", "sp"), P("dp", "sp")),
        check_vma=False,
    )
```

profile of v0, /device:TPU:0, one launch (start us, length us, event | category | flops | bytes accessed | tf_op | source)
XLA Modules:
  0.0 433.3 jit_solution(4035622993823633458)
XLA Ops:
  11.7 1.3 pad_maximum_fusion.1
  13.1 1.3 copy.55
  14.4 7.3 %all-to-all-start = ((bf16[128,8,512]{0,2,1:T(8,128)(2,1)}), bf16[128,8,512]{0,2,1:T(8,128)(2,1)S(1)}, u32[]{:S(2)}, u32[]{:S(2)}) async-start(bf16[128,8,512]{0,2,1:T(8,128)(2,1)} %bitcast.14), calls=%async_computation | async-start | bytes 2097152 | tf_op jit(solution)/shard_map/all_to_all | solution.py:98
  21.9 42.4 %all-to-all-done = bf16[128,8,512]{0,2,1:T(8,128)(2,1)S(1)} async-done(((bf16[128,8,512]{0,2,1:T(8,128)(2,1)}), bf16[128,8,512]{0,2,1:T(8,128)(2,1)S(1)}, u32[]{:S(2)}, u32[]{:S(2)}) %all-to-all-start) | async-done | bytes 1048608 | tf_op jit(solution)/shard_map/all_to_all | solution.py:98
  66.1 39.1 %all-gather.6.cloned.1.call-done = bf16[1,1024,2048]{2,1,0:T(8,128)(2,1)} async-done(((bf16[1,128,2048]{2,1,0:T(8,128)(2,1)}), bf16[1,1024,2048]{2,1,0:T(8,128)(2,1)}) %all-gather.6.cloned.1.call-update) | async-done | bytes 4194320 | tf_op jit(solution)/shard_map/all_gather | solution.py:99
  105.1 46.5 %all-gather.4.cloned.1.call-done = bf16[2048,3,512]{0,2,1:T(8,128)(2,1)} async-done(((bf16[512,3,512]{0,2,1:T(8,128)(2,1)}), bf16[2048,3,512]{0,2,1:T(8,128)(2,1)}) %all-gather.4.cloned.1.call-update) | async-done | bytes 6291472 | tf_op jit(solution)/shard_map/all_gather | solution.py:96
  151.6 10.1 %fusion.93 = bf16[1024,1536]{0,1:T(8,128)(2,1)S(1)} fusion(bf16[2048,1536]{0,1:T(8,128)(2,1)} %bitcast.197, bf16[1,1024,2048]{2,1,0:T(8,128)(2,1)} %all-gather.6.cloned.1.call-done), kind=kOutput, calls=%fused_computation.98 | convolution fusion | flops 6444023808 | bytes 13631488 | tf_op jit(solution)/shard_map/dot_general | solution.py:100
  161.7 1.5 fusion.101
  163.4 2.3 copy.54
  165.6 2.3 copy.59
  167.9 1.3 copy.53
  171.6 33.4 %while.38 = (s32[]{:T(128)}, f32[2,256,256]{2,1,0:T(8,128)S(1)}, bf16[8,2,128,256]{3,2,0,1:T(8,128)(2,1)}, bf16[8,2,128,128]{3,2,1,0:T(8,128)(2,1)}, f32[2]{0:T(...) while((s32[]{:T(128)}, f32[2,256,256]{2,1,0:T(8,128)S(1)}, ...), condition=%wide.region_1.2_spmd.clone.clone.clone, body=%wide.region_0.1_spmd.clone.clone.clone.sunk | while | flops 101646848 | bytes 3434148 | solution.py:69
  171.6 1.7 bitcast_dynamic-update-slice_fusion.2
  175.8 1.7 bitcast_dynamic-update-slice_fusion.2
  179.9 1.7 bitcast_dynamic-update-slice_fusion.2
  184.1 1.7 bitcast_dynamic-update-slice_fusion.2
  188.3 1.7 bitcast_dynamic-update-slice_fusion.2
  192.5 1.7 bitcast_dynamic-update-slice_fusion.2
  196.7 1.7 bitcast_dynamic-update-slice_fusion.2
  200.8 1.7 bitcast_dynamic-update-slice_fusion.2
  205.0 2.3 copy.63
  209.4 52.0 %while.39 = (s32[]{:T(128)}, f32[2,256,256]{2,1,0:T(8,128)S(1)}, bf16[8,2,128,256]{3,2,0,1:T(8,128)(2,1)}, bf16[8,2,128,256]{3,2,0,1:T(8,128)(2,1)}, f32[2]{0:T(...) while((s32[]{:T(128)}, f32[2,256,256]{2,1,0:T(8,128)S(1)}, ...), condition=%wide.region_3.4_spmd.clone.clone.clone, body=%wide.region_2.3_spmd.clone.clone.clone.sunk | while | flops 152306176 | bytes 4880578 | solution.py:70
  212.8 1.8 fusion.138
  215.9 1.3 fusion.139
  219.3 1.8 fusion.138
  222.4 1.3 fusion.139
  225.8 1.8 fusion.138
  228.9 1.3 fusion.139
  232.3 1.8 fusion.138
  235.4 1.3 fusion.139
  238.8 1.8 fusion.138
  241.9 1.3 fusion.139
  245.4 1.8 fusion.138
  248.4 1.3 fusion.139
  251.9 1.8 fusion.138
  254.9 1.3 fusion.139
  258.4 1.8 fusion.138
  261.4 1.6 copy.70
  263.0 1.5 copy.72
  264.5 1.3 copy.62
  265.9 10.4 %fusion.86 = bf16[2048,1536]{0,1:T(8,128)(2,1)} fusion(bf16[1,1024,2048]{2,1,0:T(8,128)(2,1)} %all-gather.6.cloned.1.call-done, bf16[1024,512]{0,1:T(8,128)(2,1)S(1)} %bitcast.193, bf16[1024,512]{0,1:T(8,128)(2,1)S(1)} %bitcast.191, bf16[1024,512]{0,1:T(8,128)(2,1)} %bitcast.195), kind=kOutput, calls=%fused_computation.92 | convolution fusion | flops 6455033856 | bytes 13631488 | tf_op jit(solution)/shard_map/dot_general | solution.py:118
  277.5 11.1 %convolution_convert_fusion.1 = bf16[1024,2048]{1,0:T(8,128)(2,1)} fusion(bf16[2048,1536]{0,1:T(8,128)(2,1)} %bitcast.198, bf16[1024,512]{0,1:T(8,128)(2,1)S(1)} %bitcast.194, bf16[1024,512]{0,1:T(8,128)(2,1)S(1)} %bitcast.192, bf16[1024,512]{0,1:T(8,128)(2,1)S(1)} %bitcast.196), kind=kOutput, calls=%fused_computation.96 | convolution fusion | flops 6453985280 | bytes 13631488 | tf_op jit(solution)/shard_map/dot_general | solution.py:109
  288.7 45.7 %reduce-scatter.5.cloned.1.call-done = bf16[512,1536]{0,1:T(8,128)(2,1)} async-done(((bf16[2048,1536]{0,1:T(8,128)(2,1)}), bf16[512,1536]{0,1:T(8,128)(2,1)}) %reduce-scatter.5.cloned.1.call-update) | async-done | bytes 1572880 | tf_op jit(solution)/shard_map/reduce_scatter | solution.py:117
  334.3 1.8 convert_multiply_fusion
  336.5 1.3 copy.73
  337.8 1.3 copy.74
  339.1 1.3 copy.75
  340.4 86.3 %reduce-scatter.3.cloned.1.call-done = bf16[128,2048]{1,0:T(8,128)(2,1)} async-done(((bf16[1024,2048]{1,0:T(8,128)(2,1)}), bf16[128,2048]{1,0:T(8,128)(2,1)}) %reduce-scatter.3.cloned.1.call-update) | async-done | bytes 524304 | tf_op jit(solution)/shard_map/reduce_scatter | solution.py:108
  (101 shorter events, 60.2 us)
Async XLA Ops:
  7.2 5.9 %copy-start.1 = (bf16[1,128,4096]{2,1,0:T(8,128)(2,1)S(1)}, bf16[1,128,4096]{2,1,0:T(8,128)(2,1)}, u32[]{:S(2)}) copy-start(bf16[1,128,4096]{2,1,0:T(8,128)(2,1)} %param.11) | copy-start | bytes 3145732
  7.2 98.0 %all-gather.6.cloned.1.call-start = ((), (), s32[]{:S(2)}) async-start(), calls=%async_computation.6 | async-start | bytes 4718592 | tf_op jit(solution)/shard_map/all_gather | solution.py:99
  7.9 143.7 %all-gather.4.cloned.1.call-start = ((), (), s32[]{:S(2)}) async-start(), calls=%async_computation.3 | async-start | bytes 7864320 | tf_op jit(solution)/shard_map/all_gather | solution.py:96
  11.7 10.1 %copy-start.3 = (f32[2]{0:T(128)S(1)}, f32[2]{0:T(128)}, u32[]{:S(2)}) copy-start(f32[2]{0:T(128)} %param.15) | copy-start | bytes 28
  14.4 49.9 %all-to-all-start = ((bf16[128,8,512]{0,2,1:T(8,128)(2,1)}), bf16[128,8,512]{0,2,1:T(8,128)(2,1)S(1)}, u32[]{:S(2)}, u32[]{:S(2)}) async-start(bf16[128,8,512]{0,2,1:T(8,128)(2,1)} %bitcast.14), calls=%async_computation | async-start | bytes 2097152 | tf_op jit(solution)/shard_map/all_to_all | solution.py:98
  21.7 312.7 %reduce-scatter.5.cloned.1.call-start = ((), (), s32[]{:S(2)}) async-start(), calls=%async_computation.5 | async-start | bytes 7864320 | tf_op jit(solution)/shard_map/reduce_scatter | solution.py:117
  261.4 3.1 copy-start
  276.3 1.2 copy-start.2
  276.3 150.4 %reduce-scatter.3.cloned.1.call-start = ((), (), s32[]{:S(2)}) async-start(), calls=%async_computation.4 | async-start | bytes 4718592 | tf_op jit(solution)/shard_map/reduce_scatter | solution.py:108
Sparse Core Ops, SparseCore 0:
  10.1 94.9 all-gather.5
  106.7 44.8 all-gather.3
  276.4 57.8 reduce-scatter.4
  338.4 88.2 reduce-scatter.2
where the time goes:
time: 435 us; the launch traced here: 433 us
  waiting for transfers between devices  261 us (60%)
  matrix products  115 us (26%)
  local copies, waits for them, and re-layouts  30.6 us (7%)
  between operations  14 us (3%)
  starting transfers between devices  7.62 us (2%)
  other arithmetic  4.64 us (1%)
    reduce_scatter x1, waiting for transfers between devices, body(): lax.psum_scatter(lax.dot_general(gradients, weights, (((1,), (1,)), ((),...  86.3 us
    all_gather x1, waiting for transfers between devices, body(): gathered = lax.all_gather(stacked, 'dp', axis=0, tiled=True)  46.5 us
    reduce_scatter x1, waiting for transfers between devices, body(): lax.psum_scatter(lax.dot_general(all_rows, gradients, (((0,), (0,)), ((),...  45.7 us
    all_to_all x1, waiting for transfers between devices, body(): lax.all_to_all(mix_cotangent[0], 'sp', split_axis=1, concat_axis=0, tiled...  42.4 us
    all_gather x1, waiting for transfers between devices, body(): all_rows = lax.all_gather(own_rows, 'sp', axis=0, tiled=True)  39.1 us
    dot_general x8, matrix products, backward(): jnp.dot(value_block, state_bf.T, preferred_element_type=jnp.float32)  14.4 us
    dot_general x8, matrix products, forward(): jnp.dot(grad_block, value_block.T, preferred_element_type=jnp.float32)  13.9 us
    unnamed x18, local copies, waits for them, and re-layouts  13.7 us
  transfers between devices with their start and end apart: 5, of which 5 were waited for; matrix products, arithmetic and copies ran while one was open for 6% of the time, Pallas kernels for 0%

commit v1 on v0

v1 whole, which is shorter than its diff:
```python
import functools

import jax
import jax.numpy as jnp
from jax import lax
from jax.experimental import pallas as pl
from jax.experimental.pallas import tpu as pltpu
from jax.sharding import PartitionSpec as P

BLOCK = 128
SUBS = 2
F32 = jnp.float32
BF16 = jnp.bfloat16
MESH = pl.DeviceIdType.MESH
NT = (((1,), (1,)), ((), ()))
TN = (((0,), (0,)), ((), ()))
VMEM_LIMIT = 60 * 1024 * 1024


def dot(a, b, dims=(((1,), (0,)), ((), ()))):
    return lax.dot_general(a, b, dims, preferred_element_type=F32)


def remote(src, dst, send, recv, where):
    return pltpu.make_async_remote_copy(
        src_ref=src, dst_ref=dst, send_sem=send, recv_sem=recv, device_id=where, device_id_type=MESH
    )


def greet(targets):
    barrier = pltpu.get_barrier_semaphore()
    for where in targets:
        pl.semaphore_signal(barrier, inc=1, device_id=where, device_id_type=MESH)
    pl.semaphore_wait(barrier, len(targets))


def gather_kernel(
    n, m, h_in, c_in, wq, wk, wv, h_all, c_all, w_all,
    h_recv, h_line, h_side, c_send, c_recv, w_far, w_near, w_recv,
):
    s = lax.axis_index("sp")
    d = lax.axis_index("dp")
    z, x = s // 2, s % 2
    y, core = d // 2, d % 2
    nz, ny = n // 2, m // 2
    rows = h_in.shape[0]
    sub_rows = rows // SUBS
    depth, columns = wq.shape
    side = s + 1 - 2 * x
    mate = d + 1 - 2 * core

    def far(o):
        return ((y + o) % ny) * 2 + core

    greet(
        [{"sp": (s + k) % n} for k in range(1, n)]
        + [{"dp": mate}]
        + [{"dp": far(o)} for o in range(1, ny)]
    )

    def h_copy(src_z, src_x, sub, dest, send, own=False):
        block = src_z * 2 + src_x
        place = pl.ds(pl.multiple_of(block * rows + sub * sub_rows, sub_rows), sub_rows)
        src = h_in.at[pl.ds(sub * sub_rows, sub_rows)] if own else h_all.at[place]
        return remote(src, h_all.at[place], send, h_recv.at[block, sub], {"sp": dest})

    def w_copy(src_d, j, dest, send, own=False):
        place = w_all.at[
            pl.ds(pl.multiple_of(src_d * depth, depth), depth), pl.ds(j * columns, columns)
        ]
        return remote((wq, wk, wv)[j] if own else place, place, send, w_recv.at[src_d, j], {"dp": dest})

    def c_copy(k):
        to = (s + k) % n
        return remote(
            c_in.at[:, pl.ds(pl.multiple_of(to * columns, columns), columns)],
            c_all.at[pl.ds(pl.multiple_of(s * rows, rows), rows)],
            c_send.at[k - 1],
            c_recv.at[k - 1],
            {"sp": to},
        )

    def line(k, sub, up, own):
        source = (z - k) if up else (z + k)
        dest = (s + 2) if up else (s - 2)
        return h_copy(source, x, sub, dest, h_line.at[k, sub, int(up)], own)

    def goes(k, up):
        if up:
            return jnp.logical_and(z - k >= 0, z + 1 < nz)
        return jnp.logical_and(z + k < nz, z >= 1)

    def arrives(k, up):
        return (z - k >= 0) if up else (z + k < nz)

    for sub in range(SUBS):
        for up in (True, False):

            @pl.when(goes(0, up))
            def _():
                line(0, sub, up, True).start()

        h_copy(z, x, sub, side, h_side.at[0, sub, 0], True).start()
    for j in range(3):
        for o in range(1, ny):
            w_copy(d, j, far(o), w_far.at[o, j], True).start()
        w_copy(d, j, mate, w_near.at[0, j], True).start()
    for k in range(1, n):
        c_copy(k).start()

    h_all[pl.ds(pl.multiple_of(s * rows, rows), rows), :] = h_in[...]
    c_all[pl.ds(pl.multiple_of(s * rows, rows), rows), :] = c_in[
        :, pl.ds(pl.multiple_of(s * columns, columns), columns)
    ]
    for j, w in enumerate((wq, wk, wv)):
        w_all[pl.ds(pl.multiple_of(d * depth, depth), depth), j * columns : (j + 1) * columns] = w[...]

    def pass_weights(j):
        for o in range(1, ny):
            w_copy(far(o), j, mate, w_near.at[o, j]).wait_recv()
            w_copy(far(o), j, mate, w_near.at[o, j]).start()

    passed = 0
    for k in range(1, nz):
        for sub in range(SUBS):
            for up in (True, False):

                @pl.when(arrives(k, up))
                def _():
                    source = (z - k) if up else (z + k)
                    h_copy(source, x, sub, side, h_side.at[k, sub, int(up)]).wait_recv()
                    h_copy(source, x, sub, side, h_side.at[k, sub, int(up)]).start()

                @pl.when(goes(k, up))
                def _():
                    line(k, sub, up, False).start()

        if passed < 3:
            pass_weights(passed)
            passed += 1
    for j in range(passed, 3):
        pass_weights(j)

    for j in range(3):
        w_copy(mate, j, mate, w_near.at[0, j]).wait_recv()
        for o in range(1, ny):
            other = far(o) + 1 - 2 * core
            w_copy(other, j, mate, w_near.at[o, j]).wait_recv()
    for zz in range(nz):
        for sub in range(SUBS):
            h_copy(zz, 1 - x, sub, side, h_side.at[0, sub, 0]).wait_recv()
    for k in range(1, n):
        c_copy(k).wait_recv()
    for k in range(1, n):
        c_copy(k).wait_send()
    for j in range(3):
        for o in range(ny):
            w_copy(d, j, mate, w_near.at[o, j]).wait_send()
            if o:
                w_copy(d, j, far(o), w_far.at[o, j]).wait_send()
    for sub in range(SUBS):
        h_copy(z, x, sub, side, h_side.at[0, sub, 0]).wait_send()
        for up in (True, False):
            for k in range(nz):

                @pl.when(goes(k, up))
                def _():
                    line(k, sub, up, False).wait_send()

                if k:

                    @pl.when(arrives(k, up))
                    def _():
                        h_copy(z, x, sub, side, h_side.at[k, sub, int(up)]).wait_send()


def gather(n, m, h, c, wq, wk, wv):
    rows, width = h.shape
    depth, columns = wq.shape
    vmem = pl.BlockSpec(memory_space=pltpu.VMEM)
    dma = pltpu.SemaphoreType.DMA
    return pl.pallas_call(
        functools.partial(gather_kernel, n, m),
        out_shape=(
            jax.ShapeDtypeStruct((rows * n, width), BF16),
            jax.ShapeDtypeStruct((rows * n, columns), BF16),
            jax.ShapeDtypeStruct((depth * m, 3 * columns), BF16),
        ),
        in_specs=[vmem] * 5,
        out_specs=(vmem,) * 3,
        scratch_shapes=[
            dma((n, SUBS)),
            dma((n // 2, SUBS, 2)),
            dma((n // 2, SUBS, 2)),
            dma((n - 1,)),
            dma((n - 1,)),
            dma((m // 2, 3)),
            dma((m // 2, 3)),
            dma((m, 3)),
        ],
        compiler_params=pltpu.CompilerParams(
            collective_id=0, has_side_effects=True, vmem_limit_bytes=VMEM_LIMIT
        ),
        name="gather_all",
    )(h, c, wq, wk, wv)


def mixer_kernel(heads, rate, h_all, c_all, w_all, g_all, p_all, state, back):
    length = h_all.shape[0]
    columns = c_all.shape[1]
    dim = columns // heads
    blocks = length // BLOCK
    scale = dim ** (-0.5)
    step = 2 * BLOCK if length % (2 * BLOCK) == 0 else BLOCK

    @pl.loop(0, length // step)
    def _(i):
        at = pl.ds(pl.multiple_of(i * step, step), step)
        for j in range(3):
            value = dot(h_all[at, :], w_all[:, j * columns : (j + 1) * columns]).astype(BF16)
            if j == 1:
                value = (value.astype(F32) * scale).astype(BF16)
            p_all[at, j * columns : (j + 1) * columns] = value

    row = lax.broadcasted_iota(jnp.int32, (BLOCK, BLOCK), 0).astype(F32)
    col = lax.broadcasted_iota(jnp.int32, (BLOCK, BLOCK), 1).astype(F32)
    place = lax.broadcasted_iota(jnp.int32, (BLOCK, dim), 0).astype(F32)
    spread = row - col
    state[...] = jnp.zeros_like(state)
    back[...] = jnp.zeros_like(back)

    @pl.loop(0, blocks)
    def _(i):
        for h in range(heads):
            g = rate[h]
            inner = jnp.where(spread >= 0, jnp.exp(g * jnp.maximum(spread, 0.0)), 0.0)
            inner_t = jnp.where(spread <= 0, jnp.exp(g * jnp.maximum(-spread, 0.0)), 0.0)
            query_decay = jnp.exp(g * (place + 1.0))
            key_decay = jnp.exp(g * (BLOCK - 1.0 - place))
            block_decay = jnp.exp(jnp.full((1, dim), g * BLOCK, F32))
            parts = [slice(j * columns + h * dim, j * columns + (h + 1) * dim) for j in range(3)]

            at = pl.ds(pl.multiple_of(i * BLOCK, BLOCK), BLOCK)
            k, v = p_all[at, parts[1]], p_all[at, parts[2]]
            c = c_all[at, parts[0]]
            mixed = (dot(c, v, NT) * inner).astype(BF16)
            held = state[h]
            grad_q = dot(mixed, k) + dot(c, held.astype(BF16), NT) * query_decay
            weighted = (k.astype(F32) * key_decay).astype(BF16)
            state[h] = held * block_decay + dot(weighted, v, TN)
            g_all[at, parts[0]] = grad_q.astype(BF16)

            at = pl.ds(pl.multiple_of((blocks - 1 - i) * BLOCK, BLOCK), BLOCK)
            q, k, v = (p_all[at, part] for part in parts)
            c = c_all[at, parts[0]]
            mixed_t = (dot(v, c, NT) * inner_t).astype(BF16)
            scores_t = (dot(k, q, NT) * inner_t).astype(BF16)
            held = back[h]
            held_bf = held.astype(BF16)
            grad_v = dot(scores_t, c) + dot(k, held_bf) * key_decay
            grad_k = (dot(mixed_t, q) + dot(v, held_bf, NT) * key_decay) * scale
            weighted = (q.astype(F32) * query_decay).astype(BF16)
            back[h] = held * block_decay + dot(weighted, c, TN)
            g_all[at, parts[1]] = grad_k.astype(BF16)
            g_all[at, parts[2]] = grad_v.astype(BF16)


def mixer(rate, h_all, c_all, w_all):
    heads = rate.shape[0]
    length = h_all.shape[0]
    width = w_all.shape[1]
    dim = c_all.shape[1] // heads
    vmem = pl.BlockSpec(memory_space=pltpu.VMEM)
    return pl.pallas_call(
        functools.partial(mixer_kernel, heads),
        out_shape=jax.ShapeDtypeStruct((length, width), BF16),
        in_specs=[pl.BlockSpec(memory_space=pltpu.SMEM), vmem, vmem, vmem],
        out_specs=vmem,
        scratch_shapes=[
            pltpu.VMEM((length, width), BF16),
            pltpu.VMEM((heads, dim, dim), F32),
            pltpu.VMEM((heads, dim, dim), F32),
        ],
        compiler_params=pltpu.CompilerParams(vmem_limit_bytes=VMEM_LIMIT),
        name="mixer",
    )(rate, h_all, c_all, w_all)


def scatter_kernel(
    n, m, h_all, w_all, g_all, dh, dq, dk, dv,
    part, ring, turned, near_out, near_in, far_out, far_in,
    r_send, r_recv, n_send, n_recv, f_send, f_recv,
):
    s = lax.axis_index("sp")
    d = lax.axis_index("dp")
    z, x = s // 2, s % 2
    y, core = d // 2, d % 2
    nz, ny = n // 2, m // 2
    rows, width = dh.shape
    depth, columns = dq.shape
    half = rows // 2
    sub_rows = half // SUBS
    mate = d + 1 - 2 * core
    me = x * (n - 1 - z) + (1 - x) * z

    def at_ring(p):
        p = (p + 2 * n) % n
        hi = p // nz
        return (hi * (n - 1 - p) + (1 - hi) * p) * 2 + hi

    def far(o):
        return ((y + o) % ny) * 2 + core

    right, left = at_ring(me + 1), at_ring(me - 1)
    greet(
        [{"sp": right}, {"sp": left}, {"dp": mate}] + [{"dp": far(o)} for o in range(1, ny)]
    )

    def own(offset):
        return pl.multiple_of(at_ring(me + offset) * rows, rows)

    ready = set()

    def compute(offset):
        offset = offset % n
        if offset in ready:
            return
        ready.add(offset)
        base = own(offset)
        chunk = width // 4

        @pl.loop(0, 4)
        def _(i):
            at = pl.ds(pl.multiple_of(i * chunk, chunk), chunk)
            part[pl.ds(base, rows), at] = dot(g_all[pl.ds(base, rows), :], w_all[at, :], NT).astype(BF16)

    def r_copy(step, way, sub):
        lane = (slice(0, half), slice(half, rows))[way].start + sub * sub_rows
        if step == 0:
            base = own(-1 if way == 0 else 1)
            src = part.at[pl.ds(pl.multiple_of(base + lane, sub_rows), sub_rows)]
        else:
            src = ring.at[step - 1, way, sub]
        return remote(
            src,
            ring.at[step, way, sub],
            r_send.at[step, way, sub],
            r_recv.at[step, way, sub],
            {"sp": right if way == 0 else left},
        )

    def process(step):
        for sub in range(SUBS):
            for way in range(2):
                base = own(-(step + 2) if way == 0 else step + 2)
                lane = way * half + sub * sub_rows
                r_copy(step, way, sub).wait_recv()
                mine = part[pl.ds(pl.multiple_of(base + lane, sub_rows), sub_rows), :]
                total = (ring[step, way, sub].astype(F32) + mine.astype(F32)).astype(BF16)
                if step < n - 2:
                    ring[step, way, sub] = total
                    r_copy(step + 1, way, sub).start()
                else:
                    dh[lane : lane + sub_rows, :] = total

    def turn(device):
        turned[...] = h_all[:, pl.ds(pl.multiple_of(device * depth, depth), depth)].T

    def weight_part(j):
        return dot(turned[...], g_all[:, pl.ds(pl.multiple_of(j * columns, columns), columns)])

    def n_copy(o):
        return remote(near_out.at[o], near_in.at[o], n_send.at[o], n_recv.at[o], {"dp": mate})

    def f_copy(o, j):
        return remote(
            far_out.at[o - 1, j], far_in.at[o - 1, j], f_send.at[o - 1, j], f_recv.at[o - 1, j], {"dp": far(o)}
        )

    def near(o):
        turn(far(o) + 1 - 2 * core)

        @pl.loop(0, 3)
        def _(j):
            near_out[o, j] = weight_part(j).astype(BF16)

        n_copy(o).start()

    def chip_sum(o):
        turn(far(o))
        n_copy(o).wait_recv()
        if o:
            for j in range(3):
                far_out[o - 1, j] = (weight_part(j) + near_in[o, j].astype(F32)).astype(BF16)
                f_copy(o, j).start()
        else:
            for j, out in enumerate((dq, dk, dv)):
                out[...] = weight_part(j) + near_in[o, j].astype(F32)

    tasks = []
    for o in range(1, ny):
        tasks += [functools.partial(near, o), functools.partial(chip_sum, o)]
    tasks += [functools.partial(near, 0), functools.partial(chip_sum, 0)]

    compute(-1)
    for sub in range(SUBS):
        r_copy(0, 0, sub).start()
    compute(1)
    for sub in range(SUBS):
        r_copy(0, 1, sub).start()
    for step in range(n - 1):
        if tasks:
            tasks.pop(0)()
        compute(-(step + 2))
        compute(step + 2)
        process(step)
    while tasks:
        tasks.pop(0)()
    for j, out in enumerate((dq, dk, dv)):
        total = out[...]
        for o in range(1, ny):
            f_copy(o, j).wait_recv()
            total = total + far_in[o - 1, j].astype(F32)
        out[...] = total * (1.0 / m)
    for step in range(n - 1):
        for sub in range(SUBS):
            for way in range(2):
                r_copy(step, way, sub).wait_send()
    for o in range(ny):
        n_copy(o).wait_send()
        if o:
            for j in range(3):
                f_copy(o, j).wait_send()


def scatter(n, m, h_all, w_all, g_all):
    length, width = h_all.shape
    rows = length // n
    depth = width // m
    columns = w_all.shape[1] // 3
    ny = m // 2
    vmem = pl.BlockSpec(memory_space=pltpu.VMEM)
    dma = pltpu.SemaphoreType.DMA
    sub_rows = rows // 2 // SUBS
    return pl.pallas_call(
        functools.partial(scatter_kernel, n, m),
        out_shape=(jax.ShapeDtypeStruct((rows, width), BF16),)
        + (jax.ShapeDtypeStruct((depth, columns), F32),) * 3,
        in_specs=[vmem] * 3,
        out_specs=(vmem,) * 4,
        scratch_shapes=[
            pltpu.VMEM((length, width), BF16),
            pltpu.VMEM((n - 1, 2, SUBS, sub_rows, width), BF16),
            pltpu.VMEM((depth, length), BF16),
            pltpu.VMEM((ny, 3, depth, columns), BF16),
            pltpu.VMEM((ny, 3, depth, columns), BF16),
            pltpu.VMEM((ny - 1, 3, depth, columns), BF16),
            pltpu.VMEM((ny - 1, 3, depth, columns), BF16),
            dma((n - 1, 2, SUBS)),
            dma((n - 1, 2, SUBS)),
            dma((ny,)),
            dma((ny,)),
            dma((ny - 1, 3)),
            dma((ny - 1, 3)),
        ],
        compiler_params=pltpu.CompilerParams(
            collective_id=1, has_side_effects=True, vmem_limit_bytes=VMEM_LIMIT
        ),
        name="scatter_all",
    )(h_all, w_all, g_all)


def body(n, m, hidden_in, mix_cotangent, query_weight, key_weight, value_weight, decay_log):
    h_all, c_all, w_all = gather(
        n, m, hidden_in[0], mix_cotangent[0], query_weight, key_weight, value_weight
    )
    g_all = mixer(decay_log, h_all, c_all, w_all)
    dh, dq, dk, dv = scatter(n, m, h_all, w_all, g_all)
    return dh[None], dq, dk, dv


def solution(mesh):
    placed = (
        P("dp", "sp", None),
        P("dp", "sp", None),
        P("dp", "sp"),
        P("dp", "sp"),
        P("dp", "sp"),
        P("sp"),
    )
    return jax.shard_map(
        functools.partial(body, mesh.shape["sp"], mesh.shape["dp"]),
        mesh=mesh,
        in_specs=placed,
        out_specs=(P("dp", "sp", None), P("dp", "sp"), P("dp", "sp"), P("dp", "sp")),
        check_vma=False,
    )
```

time: 435 us -> 158 us (0.36)
  waiting for transfers between devices: 261 us -> 0 us
  Pallas kernels: 0 us -> 150 us
  matrix products: 115 us -> 0 us
  local copies, waits for them, and re-layouts: 30.6 us -> 7.47 us
  between operations: 14 us -> 0.66 us
  starting transfers between devices: 7.62 us -> 0 us
  other arithmetic: 4.64 us -> 0 us
    pallas_call x0 -> x3, Pallas kernels: none -> 150 us  [the longest x1 70.5 us: gather(): pl.pallas_call(functools.partial(gather_kernel, n, m), out_shape=(jax.Sha...]
    reduce_scatter x2 -> x0, waiting for transfers between devices: 132 us -> none  [the longest x1 86.3 us: body(): lax.psum_scatter(lax.dot_general(gradients, weights, (((1,), (1,)), ((),...]
    dot_general x75 -> x0, matrix products: 115 us -> none  [the longest x8 14.4 us: backward(): jnp.dot(value_block, state_bf.T, preferred_element_type=jnp.float32)]
    all_gather x2 -> x0, waiting for transfers between devices: 85.5 us -> none  [the longest x1 46.5 us: body(): gathered = lax.all_gather(stacked, 'dp', axis=0, tiled=True)]
    all_to_all x1 -> x0, waiting for transfers between devices: 42.4 us -> none  [body(): lax.all_to_all(mix_cotangent[0], 'sp', split_axis=1, concat_axis=0, tiled...]
    all_to_all x1 -> x0, starting transfers between devices: 7.28 us -> none  [body(): lax.all_to_all(mix_cotangent[0], 'sp', split_axis=1, concat_axis=0, tiled...]
    unnamed x18 -> x6, local copies, waits for them, and re-layouts: 13.7 us -> 7.47 us
    reshape x3 -> x0, local copies, waits for them, and re-layouts: 5.06 us -> none  [by_head(): return series.reshape(length, head_count, -1).transpose(1, 0, 2)]
  transfers between devices with their start and end apart: 5 -> 0, of which waited for: 5 -> 0; matrix products, arithmetic and copies ran while one was open for 6% -> 0% of each run, Pallas kernels for 0% -> 0%
where the time goes in v1:
time: 158 us
  Pallas kernels  150 us (95%)
  local copies, waits for them, and re-layouts  7.47 us (5%)
    pallas_call x1, Pallas kernels, gather(): pl.pallas_call(functools.partial(gather_kernel, n, m), out_shape=(jax.Sha...  70.5 us
    pallas_call x1, Pallas kernels, scatter(): pl.pallas_call(functools.partial(scatter_kernel, n, m), out_shape=(jax.Sh...  59.4 us
    pallas_call x1, Pallas kernels, mixer(): pl.pallas_call(functools.partial(mixer_kernel, heads), out_shape=jax.Shap...  20 us
    unnamed x6, local copies, waits for them, and re-layouts  7.47 us

profile of v1, /device:TPU:0, one launch (start us, length us, event | category | flops | bytes accessed | tf_op | source)
XLA Modules:
  0.0 158.0 jit_solution(15094572126795931925)
XLA Ops:
  0.6 70.5 %gather_all.1 = (bf16[1024,2048]{1,0:T(8,128)(2,1)}, bf16[1024,512]{1,0:T(8,128)(2,1)}, bf16[2048,1536]{1,0:T(8,128)(2,1)}) custom-call(bf16[128,2048]{1,0:T(8,128)(2,1)} %bitcast.5, bf16[128,4096]{1,0:T(8,128)(2,1)} %bitcast.3, bf16[512,512]{1,0:T(8,128)(2,1)} %wq.1, bf16[512,512]{1,0:T(8,128)(2,1)} %wk.1, bf16[512,512]{1,0:T(8,128)(2,1)} %wv.1), custom_call_target="tpu_custom_call" | custom-call | tf_op jit(solution)/shard_map/gather_all/pallas_call | solution.py:182
  71.1 20.0 %mixer.1.g_all = bf16[1024,1536]{1,0:T(8,128)(2,1)} custom-call(f32[2]{0:T(128)} %rate.1, bf16[1024,2048]{1,0:T(8,128)(2,1)} %get-tuple-element.11.h_all, bf16[1024,512]{1,0:T(8,128)(2,1)} %get-tuple-element.13.c_all, bf16[2048,1536]{1,0:T(8,128)(2,1)} %get-tuple-element.12.w_all), custom_call_target="tpu_custom_call" | custom-call | tf_op jit(solution)/shard_map/mixer/pallas_call | solution.py:274
  91.1 59.4 %scatter_all.1 = (bf16[128,2048]{1,0:T(8,128)(2,1)}, f32[512,512]{1,0:T(8,128)}, f32[512,512]{1,0:T(8,128)}, f32[512,512]{1,0:T(8,128)}) custom-call(bf16[1024,2048]{1,0:T(8,128)(2,1)} %get-tuple-element.11.h_all, bf16[2048,1536]{1,0:T(8,128)(2,1)} %get-tuple-element.12.w_all, bf16[1024,1536]{1,0:T(8,128)(2,1)} %mixer.1.g_all), custom_call_target="tpu_custom_call" | custom-call | tf_op jit(solution)/shard_map/scatter_all/pallas_call | solution.py:445
  150.5 0.0 copy-start
  150.5 2.0 %copy.14 = bf16[1,128,2048]{2,1,0:T(8,128)(2,1)} copy(bf16[1,128,2048]{2,1,0:T(8,128)(2,1)} %bitcast.4) | data formatting | bytes 1048576
  152.5 2.3 %copy.15 = f32[512,512]{1,0:T(8,128)} copy(f32[512,512]{1,0:T(8,128)} %get-tuple-element.23) | data formatting | bytes 2097152
  154.8 2.3 %copy.16 = f32[512,512]{1,0:T(8,128)} copy(f32[512,512]{1,0:T(8,128)} %get-tuple-element.24) | data formatting | bytes 2097152
  157.0 0.0 copy-done
  157.0 1.0 copy.17
Async XLA Ops:
  150.5 6.5 %copy-start = (f32[512,512]{1,0:T(8,128)S(1)}, f32[512,512]{1,0:T(8,128)}, u32[]{:S(2)}) copy-start(f32[512,512]{1,0:T(8,128)} %get-tuple-element.25) | copy-start | bytes 3145732

commit v2 on v1

--- a/solution.py
+++ b/solution.py
@@ -14,7 +14,7 @@
 MESH = pl.DeviceIdType.MESH
 NT = (((1,), (1,)), ((), ()))
 TN = (((0,), (0,)), ((), ()))
-VMEM_LIMIT = 60 * 1024 * 1024
+VMEM_LIMIT = 56 * 1024 * 1024
 
 
 def dot(a, b, dims=(((1,), (0,)), ((), ()))):
@@ -34,8 +34,8 @@
     pl.semaphore_wait(barrier, len(targets))
 
 
-def gather_kernel(
-    n, m, h_in, c_in, wq, wk, wv, h_all, c_all, w_all,
+def gather_phase(
+    n, m, project, h_in, c_in, wq, wk, wv, h_all, c_all, w_all,
     h_recv, h_line, h_side, c_send, c_recv, w_far, w_near, w_recv,
 ):
     s = lax.axis_index("sp")
@@ -105,8 +105,6 @@
         for o in range(1, ny):
             w_copy(d, j, far(o), w_far.at[o, j], True).start()
         w_copy(d, j, mate, w_near.at[0, j], True).start()
-    for k in range(1, n):
-        c_copy(k).start()
 
     h_all[pl.ds(pl.multiple_of(s * rows, rows), rows), :] = h_in[...]
     c_all[pl.ds(pl.multiple_of(s * rows, rows), rows), :] = c_in[
@@ -120,6 +118,12 @@
             w_copy(far(o), j, mate, w_near.at[o, j]).wait_recv()
             w_copy(far(o), j, mate, w_near.at[o, j]).start()
 
+    def send_cotangent():
+        for hop in range(1, n):
+            c_copy(hop).start()
+
+    if nz < 2:
+        send_cotangent()
     passed = 0
     for k in range(1, nz):
         for sub in range(SUBS):
@@ -135,6 +139,8 @@
                 def _():
                     line(k, sub, up, False).start()
 
+        if k == 1:
+            send_cotangent()
         if passed < 3:
             pass_weights(passed)
             passed += 1
@@ -146,82 +152,62 @@
         for o in range(1, ny):
             other = far(o) + 1 - 2 * core
             w_copy(other, j, mate, w_near.at[o, j]).wait_recv()
-    for zz in range(nz):
+
+    @pl.loop(0, nz)
+    def _(zz):
+        project(zz * 2 + x)
+
+    turn = 1 - 2 * (z // ((nz + 1) // 2))
+
+    @pl.loop(0, nz)
+    def _(k):
+        zz = (z + turn * k + nz) % nz
         for sub in range(SUBS):
             h_copy(zz, 1 - x, sub, side, h_side.at[0, sub, 0]).wait_recv()
+        project(zz * 2 + 1 - x)
+
     for k in range(1, n):
         c_copy(k).wait_recv()
-    for k in range(1, n):
-        c_copy(k).wait_send()
+    def drain():
+        for k in range(1, n):
+            c_copy(k).wait_send()
+        for j in range(3):
+            for o in range(ny):
+                w_copy(d, j, mate, w_near.at[o, j]).wait_send()
+                if o:
+                    w_copy(d, j, far(o), w_far.at[o, j]).wait_send()
+        for sub in range(SUBS):
+            h_copy(z, x, sub, side, h_side.at[0, sub, 0]).wait_send()
+            for up in (True, False):
+                for k in range(nz):
+
+                    @pl.when(goes(k, up))
+                    def _():
+                        line(k, sub, up, False).wait_send()
+
+                    if k:
+
+                        @pl.when(arrives(k, up))
+                        def _():
+                            h_copy(z, x, sub, side, h_side.at[k, sub, int(up)]).wait_send()
+
+    return drain
+
+
+def project_block(h_all, w_all, p_all, rows, columns, scale, block):
+    at = pl.ds(pl.multiple_of(block * rows, rows), rows)
     for j in range(3):
-        for o in range(ny):
-            w_copy(d, j, mate, w_near.at[o, j]).wait_send()
-            if o:
-                w_copy(d, j, far(o), w_far.at[o, j]).wait_send()
-    for sub in range(SUBS):
-        h_copy(z, x, sub, side, h_side.at[0, sub, 0]).wait_send()
-        for up in (True, False):
-            for k in range(nz):
-
-                @pl.when(goes(k, up))
-                def _():
-                    line(k, sub, up, False).wait_send()
-
-                if k:
-
-                    @pl.when(arrives(k, up))
-                    def _():
-                        h_copy(z, x, sub, side, h_side.at[k, sub, int(up)]).wait_send()
-
-
-def gather(n, m, h, c, wq, wk, wv):
-    rows, width = h.shape
-    depth, columns = wq.shape
-    vmem = pl.BlockSpec(memory_space=pltpu.VMEM)
-    dma = pltpu.SemaphoreType.DMA
-    return pl.pallas_call(
-        functools.partial(gather_kernel, n, m),
-        out_shape=(
-            jax.ShapeDtypeStruct((rows * n, width), BF16),
-            jax.ShapeDtypeStruct((rows * n, columns), BF16),
-            jax.ShapeDtypeStruct((depth * m, 3 * columns), BF16),
-        ),
-        in_specs=[vmem] * 5,
-        out_specs=(vmem,) * 3,
-        scratch_shapes=[
-            dma((n, SUBS)),
-            dma((n // 2, SUBS, 2)),
-            dma((n // 2, SUBS, 2)),
-            dma((n - 1,)),
-            dma((n - 1,)),
-            dma((m // 2, 3)),
-            dma((m // 2, 3)),
-            dma((m, 3)),
-        ],
-        compiler_params=pltpu.CompilerParams(
-            collective_id=0, has_side_effects=True, vmem_limit_bytes=VMEM_LIMIT
-        ),
-        name="gather_all",
-    )(h, c, wq, wk, wv)
-
-
-def mixer_kernel(heads, rate, h_all, c_all, w_all, g_all, p_all, state, back):
-    length = h_all.shape[0]
-    columns = c_all.shape[1]
+        value = dot(h_all[at, :], w_all[:, j * columns : (j + 1) * columns]).astype(BF16)
+        if j == 1:
+            value = (value.astype(F32) * scale).astype(BF16)
+        p_all[at, j * columns : (j + 1) * columns] = value
+
+
+def mixer_phase(heads, rate, c_all, p_all, g_all, state, back):
+    length, columns = c_all.shape
     dim = columns // heads
     blocks = length // BLOCK
     scale = dim ** (-0.5)
-    step = 2 * BLOCK if length % (2 * BLOCK) == 0 else BLOCK
-
-    @pl.loop(0, length // step)
-    def _(i):
-        at = pl.ds(pl.multiple_of(i * step, step), step)
-        for j in range(3):
-            value = dot(h_all[at, :], w_all[:, j * columns : (j + 1) * columns]).astype(BF16)
-            if j == 1:
-                value = (value.astype(F32) * scale).astype(BF16)
-            p_all[at, j * columns : (j + 1) * columns] = value
-
     row = lax.broadcasted_iota(jnp.int32, (BLOCK, BLOCK), 0).astype(F32)
     col = lax.broadcasted_iota(jnp.int32, (BLOCK, BLOCK), 1).astype(F32)
     place = lax.broadcasted_iota(jnp.int32, (BLOCK, dim), 0).astype(F32)
@@ -265,28 +251,7 @@
             g_all[at, parts[2]] = grad_v.astype(BF16)
 
 
-def mixer(rate, h_all, c_all, w_all):
-    heads = rate.shape[0]
-    length = h_all.shape[0]
-    width = w_all.shape[1]
-    dim = c_all.shape[1] // heads
-    vmem = pl.BlockSpec(memory_space=pltpu.VMEM)
-    return pl.pallas_call(
-        functools.partial(mixer_kernel, heads),
-        out_shape=jax.ShapeDtypeStruct((length, width), BF16),
-        in_specs=[pl.BlockSpec(memory_space=pltpu.SMEM), vmem, vmem, vmem],
-        out_specs=vmem,
-        scratch_shapes=[
-            pltpu.VMEM((length, width), BF16),
-            pltpu.VMEM((heads, dim, dim), F32),
-            pltpu.VMEM((heads, dim, dim), F32),
-        ],
-        compiler_params=pltpu.CompilerParams(vmem_limit_bytes=VMEM_LIMIT),
-        name="mixer",
-    )(rate, h_all, c_all, w_all)
-
-
-def scatter_kernel(
+def scatter_phase(
     n, m, h_all, w_all, g_all, dh, dq, dk, dv,
     part, ring, turned, near_out, near_in, far_out, far_in,
     r_send, r_recv, n_send, n_recv, f_send, f_recv,
@@ -312,27 +277,29 @@
         return ((y + o) % ny) * 2 + core
 
     right, left = at_ring(me + 1), at_ring(me - 1)
-    greet(
-        [{"sp": right}, {"sp": left}, {"dp": mate}] + [{"dp": far(o)} for o in range(1, ny)]
-    )
 
     def own(offset):
         return pl.multiple_of(at_ring(me + offset) * rows, rows)
 
     ready = set()
 
-    def compute(offset):
-        offset = offset % n
-        if offset in ready:
+    def compute(*offsets):
+        todo = []
+        for offset in offsets:
+            if offset % n not in ready:
+                ready.add(offset % n)
+                todo.append(own(offset))
+        if not todo:
             return
-        ready.add(offset)
-        base = own(offset)
         chunk = width // 4
 
         @pl.loop(0, 4)
         def _(i):
             at = pl.ds(pl.multiple_of(i * chunk, chunk), chunk)
-            part[pl.ds(base, rows), at] = dot(g_all[pl.ds(base, rows), :], w_all[at, :], NT).astype(BF16)
+            lhs = jnp.concatenate([g_all[pl.ds(base, rows), :] for base in todo], axis=0)
+            value = dot(lhs, w_all[at, :], NT).astype(BF16)
+            for spot, base in enumerate(todo):
+                part[pl.ds(base, rows), at] = value[spot * rows : (spot + 1) * rows]
 
     def r_copy(step, way, sub):
         lane = (slice(0, half), slice(half, rows))[way].start + sub * sub_rows
@@ -402,18 +369,22 @@
         tasks += [functools.partial(near, o), functools.partial(chip_sum, o)]
     tasks += [functools.partial(near, 0), functools.partial(chip_sum, 0)]
 
-    compute(-1)
+    compute(-1, 1)
     for sub in range(SUBS):
-        r_copy(0, 0, sub).start()
-    compute(1)
-    for sub in range(SUBS):
-        r_copy(0, 1, sub).start()
+        for way in range(2):
+            r_copy(0, way, sub).start()
     for step in range(n - 1):
-        if tasks:
+        early = step % 2 == 0
+        if early and tasks:
             tasks.pop(0)()
-        compute(-(step + 2))
-        compute(step + 2)
+        compute(-(step + 2), step + 2)
         process(step)
+        if not early and tasks:
+            tasks.pop(0)()
+        if step == 0 and tasks:
+            tasks.pop(0)()
+        if step + 3 == n // 2:
+            compute(n // 2, 0)
     while tasks:
         tasks.pop(0)()
     for j, out in enumerate((dq, dk, dv)):
@@ -433,22 +404,53 @@
                 f_copy(o, j).wait_send()
 
 
-def scatter(n, m, h_all, w_all, g_all):
-    length, width = h_all.shape
-    rows = length // n
-    depth = width // m
-    columns = w_all.shape[1] // 3
+def whole_kernel(n, m, heads, rate, h_in, c_in, wq, wk, wv, dh, dq, dk, dv, *scratch):
+    h_all, c_all, w_all, p_all, g_all, state, back = scratch[:7]
+    gather_sems, rest = scratch[7:15], scratch[15:]
+    columns = wq.shape[1]
+    project = functools.partial(
+        project_block, h_all, w_all, p_all, h_in.shape[0], columns, (columns // heads) ** (-0.5)
+    )
+    drain = gather_phase(
+        n, m, project, h_in, c_in, wq, wk, wv, h_all, c_all, w_all, *gather_sems
+    )
+    mixer_phase(heads, rate, c_all, p_all, g_all, state, back)
+    scatter_phase(n, m, h_all, w_all, g_all, dh, dq, dk, dv, *rest)
+    drain()
+
+
+def whole(n, m, rate, h, c, wq, wk, wv):
+    rows, width = h.shape
+    depth, columns = wq.shape
+    heads = rate.shape[0]
+    dim = columns // heads
+    length = rows * n
     ny = m // 2
     vmem = pl.BlockSpec(memory_space=pltpu.VMEM)
     dma = pltpu.SemaphoreType.DMA
     sub_rows = rows // 2 // SUBS
     return pl.pallas_call(
-        functools.partial(scatter_kernel, n, m),
+        functools.partial(whole_kernel, n, m, heads),
         out_shape=(jax.ShapeDtypeStruct((rows, width), BF16),)
         + (jax.ShapeDtypeStruct((depth, columns), F32),) * 3,
-        in_specs=[vmem] * 3,
+        in_specs=[pl.BlockSpec(memory_space=pltpu.SMEM)] + [vmem] * 5,
         out_specs=(vmem,) * 4,
         scratch_shapes=[
+            pltpu.VMEM((length, width), BF16),
+            pltpu.VMEM((length, columns), BF16),
+            pltpu.VMEM((depth * m, 3 * columns), BF16),
+            pltpu.VMEM((length, 3 * columns), BF16),
+            pltpu.VMEM((length, 3 * columns), BF16),
+            pltpu.VMEM((heads, dim, dim), F32),
+            pltpu.VMEM((heads, dim, dim), F32),
+            dma((n, SUBS)),
+            dma((n // 2, SUBS, 2)),
+            dma((n // 2, SUBS, 2)),
+            dma((n - 1,)),
+            dma((n - 1,)),
+            dma((ny, 3)),
+            dma((ny, 3)),
+            dma((m, 3)),
             pltpu.VMEM((length, width), BF16),
             pltpu.VMEM((n - 1, 2, SUBS, sub_rows, width), BF16),
             pltpu.VMEM((depth, length), BF16),
@@ -464,18 +466,55 @@
             dma((ny - 1, 3)),
         ],
         compiler_params=pltpu.CompilerParams(
-            collective_id=1, has_side_effects=True, vmem_limit_bytes=VMEM_LIMIT
+            collective_id=0, has_side_effects=True, vmem_limit_bytes=VMEM_LIMIT
         ),
-        name="scatter_all",
-    )(h_all, w_all, g_all)
+        name="whole",
+    )(rate, h, c, wq, wk, wv)
+
+
+def finish_kernel(count, *refs):
+    ins, outs, held = refs[:count], refs[count : 2 * count], refs[2 * count : 3 * count]
+    sems = refs[3 * count]
+    moves = []
+    for i in range(count):
+        piece = ins[i].shape[0] // 2
+        for half in range(2):
+            at = pl.ds(half * piece, piece)
+            moves.append(
+                (
+                    pltpu.make_async_copy(ins[i].at[at], held[i].at[at], sems.at[0, i, half]),
+                    pltpu.make_async_copy(held[i].at[at], outs[i].at[at], sems.at[1, i, half]),
+                )
+            )
+    for fetch, _ in moves:
+        fetch.start()
+    for fetch, put in moves:
+        fetch.wait()
+        put.start()
+    for _, put in moves:
+        put.wait()
+
+
+def finish(*arrays):
+    spec = pl.BlockSpec(memory_space=pl.ANY)
+    count = len(arrays)
+    return pl.pallas_call(
+        functools.partial(finish_kernel, count),
+        out_shape=tuple(jax.ShapeDtypeStruct(a.shape, a.dtype) for a in arrays),
+        in_specs=[spec] * count,
+        out_specs=(spec,) * count,
+        scratch_shapes=[pltpu.VMEM(a.shape, a.dtype) for a in arrays]
+        + [pltpu.SemaphoreType.DMA((2, count, 2))],
+        name="finish",
+    )(*arrays)
 
 
 def body(n, m, hidden_in, mix_cotangent, query_weight, key_weight, value_weight, decay_log):
-    h_all, c_all, w_all = gather(
-        n, m, hidden_in[0], mix_cotangent[0], query_weight, key_weight, value_weight
-    )
-    g_all = mixer(decay_log, h_all, c_all, w_all)
-    dh, dq, dk, dv = scatter(n, m, h_all, w_all, g_all)
+    dh, dq, dk, dv = finish(
+        *whole(
+            n, m, decay_log, hidden_in[0], mix_cotangent[0], query_weight, key_weight, value_weight
+        )
+    )
     return dh[None], dq, dk, dv
 
 

time: 158 us -> 130 us (0.82)
  Pallas kernels: 150 us -> 130 us
  local copies, waits for them, and re-layouts: 7.47 us -> 0 us
    pallas_call x3 -> x2, Pallas kernels: 150 us -> 130 us  [the longest x1 126 us: whole(): pl.pallas_call(functools.partial(whole_kernel, n, m, heads), out_shape=(j...]
    unnamed x6 -> x0, local copies, waits for them, and re-layouts: 7.47 us -> none
where the time goes in v2:
time: 130 us
  Pallas kernels  130 us (100%)
    pallas_call x1, Pallas kernels, whole(): pl.pallas_call(functools.partial(whole_kernel, n, m, heads), out_shape=(j...  126 us
    pallas_call x1, Pallas kernels, finish(): pl.pallas_call(functools.partial(finish_kernel, count), out_shape=tuple((...  3.26 us

profile of v2, /device:TPU:0, one launch (start us, length us, event | category | flops | bytes accessed | tf_op | source)
XLA Modules:
  0.0 130.2 jit_solution(13028742613137198695)
XLA Ops:
  0.6 126.3 %whole.1 = (bf16[128,2048]{1,0:T(8,128)(2,1)}, f32[512,512]{1,0:T(8,128)}, f32[512,512]{1,0:T(8,128)}, f32[512,512]{1,0:T(8,128)}) custom-call(f32[2]{0:T(128)} %rate.1, bf16[128,2048]{1,0:T(8,128)(2,1)} %bitcast.4, bf16[128,4096]{1,0:T(8,128)(2,1)} %bitcast.3, bf16[512,512]{1,0:T(8,128)(2,1)} %wq.1, bf16[512,512]{1,0:T(8,128)(2,1)} %wk.1, bf16[512,512]{1,0:T(8,128)(2,1)} %wv.1), custom_call_target="tpu_custom_call" | custom-call | tf_op jit(solution)/shard_map/whole/pallas_call | solution.py:432
  127.0 3.3 %finish.1 = (bf16[128,2048]{1,0:T(8,128)(2,1)}, f32[512,512]{1,0:T(8,128)}, f32[512,512]{1,0:T(8,128)}, f32[512,512]{1,0:T(8,128)}) custom-call(bf16[128,2048]{1,0:T(8,128)(2,1)} %get-tuple-element.12.refs_0_, f32[512,512]{1,0:T(8,128)} %get-tuple-element.13.refs_1_, f32[512,512]{1,0:T(8,128)} %get-tuple-element.14.refs_2_, f32[512,512]{1,0:T(8,128)} %get-tuple-element.15.refs_3_), custom_call_target="tpu_custom_call" | custom-call | tf_op jit(solution)/shard_map/finish/pallas_call | solution.py:501

commit v3 on v2

--- a/solution.py
+++ b/solution.py
@@ -14,7 +14,7 @@
 MESH = pl.DeviceIdType.MESH
 NT = (((1,), (1,)), ((), ()))
 TN = (((0,), (0,)), ((), ()))
-VMEM_LIMIT = 56 * 1024 * 1024
+VMEM_LIMIT = 52 * 1024 * 1024
 
 
 def dot(a, b, dims=(((1,), (0,)), ((), ()))):
@@ -122,8 +122,6 @@
         for hop in range(1, n):
             c_copy(hop).start()
 
-    if nz < 2:
-        send_cotangent()
     passed = 0
     for k in range(1, nz):
         for sub in range(SUBS):
@@ -139,11 +137,7 @@
                 def _():
                     line(k, sub, up, False).start()
 
-        if k == 1:
-            send_cotangent()
-        if passed < 3:
-            pass_weights(passed)
-            passed += 1
+    send_cotangent()
     for j in range(passed, 3):
         pass_weights(j)
 
@@ -431,8 +425,8 @@
     sub_rows = rows // 2 // SUBS
     return pl.pallas_call(
         functools.partial(whole_kernel, n, m, heads),
-        out_shape=(jax.ShapeDtypeStruct((rows, width), BF16),)
-        + (jax.ShapeDtypeStruct((depth, columns), F32),) * 3,
+        out_shape=(pltpu.VMEM((rows, width), BF16),)
+        + (pltpu.VMEM((depth, columns), F32),) * 3,
         in_specs=[pl.BlockSpec(memory_space=pltpu.SMEM)] + [vmem] * 5,
         out_specs=(vmem,) * 4,
         scratch_shapes=[
@@ -473,38 +467,23 @@
 
 
 def finish_kernel(count, *refs):
-    ins, outs, held = refs[:count], refs[count : 2 * count], refs[2 * count : 3 * count]
-    sems = refs[3 * count]
-    moves = []
-    for i in range(count):
-        piece = ins[i].shape[0] // 2
-        for half in range(2):
-            at = pl.ds(half * piece, piece)
-            moves.append(
-                (
-                    pltpu.make_async_copy(ins[i].at[at], held[i].at[at], sems.at[0, i, half]),
-                    pltpu.make_async_copy(held[i].at[at], outs[i].at[at], sems.at[1, i, half]),
-                )
-            )
-    for fetch, _ in moves:
-        fetch.start()
-    for fetch, put in moves:
-        fetch.wait()
-        put.start()
-    for _, put in moves:
-        put.wait()
+    ins, outs, sems = refs[:count], refs[count : 2 * count], refs[2 * count]
+    moves = [pltpu.make_async_copy(ins[i], outs[i], sems.at[i]) for i in range(count)]
+    for move in moves:
+        move.start()
+    for move in moves:
+        move.wait()
 
 
 def finish(*arrays):
-    spec = pl.BlockSpec(memory_space=pl.ANY)
     count = len(arrays)
     return pl.pallas_call(
         functools.partial(finish_kernel, count),
         out_shape=tuple(jax.ShapeDtypeStruct(a.shape, a.dtype) for a in arrays),
-        in_specs=[spec] * count,
-        out_specs=(spec,) * count,
-        scratch_shapes=[pltpu.VMEM(a.shape, a.dtype) for a in arrays]
-        + [pltpu.SemaphoreType.DMA((2, count, 2))],
+        in_specs=[pl.BlockSpec(memory_space=pltpu.VMEM)] * count,
+        out_specs=(pl.BlockSpec(memory_space=pl.ANY),) * count,
+        scratch_shapes=[pltpu.SemaphoreType.DMA((count,))],
+        compiler_params=pltpu.CompilerParams(vmem_limit_bytes=4 * 1024 * 1024),
         name="finish",
     )(*arrays)
 

time: 130 us -> 124 us (0.954)
  Pallas kernels: 130 us -> 123 us
    pallas_call x1, Pallas kernels: 126 us -> 121 us  [whole(): pl.pallas_call(functools.partial(whole_kernel, n, m, heads), out_shape=(p...]
    pallas_call x1, Pallas kernels: 3.26 us -> 1.87 us  [finish(): pl.pallas_call(functools.partial(finish_kernel, count), out_shape=tuple((...]
where the time goes in v3:
time: 124 us; the launch traced here: 123 us
  Pallas kernels  123 us (99%)
    pallas_call x1, Pallas kernels, whole(): pl.pallas_call(functools.partial(whole_kernel, n, m, heads), out_shape=(p...  121 us

profile of v3, /device:TPU:0, one launch (start us, length us, event | category | flops | bytes accessed | tf_op | source)
XLA Modules:
  0.0 123.5 jit_solution(72487931110630471)
XLA Ops:
  0.6 121.0 %whole.1 = (bf16[128,2048]{1,0:T(8,128)(2,1)S(1)}, f32[512,512]{1,0:T(8,128)S(1)}, f32[512,512]{1,0:T(8,128)S(1)}, f32[512,512]{1,0:T(8,128)S(1)}) custom-call(f32[2]{0:T(128)} %rate.1, bf16[128,2048]{1,0:T(8,128)(2,1)} %bitcast.4, bf16[128,4096]{1,0:T(8,128)(2,1)} %bitcast.3, bf16[512,512]{1,0:T(8,128)(2,1)} %wq.1, bf16[512,512]{1,0:T(8,128)(2,1)} %wk.1, ...), custom_call_target="tpu_custom_call" | custom-call | tf_op jit(solution)/shard_map/whole/pallas_call | solution.py:426
  121.6 1.9 %finish.1 = (bf16[128,2048]{1,0:T(8,128)(2,1)}, f32[512,512]{1,0:T(8,128)}, f32[512,512]{1,0:T(8,128)}, f32[512,512]{1,0:T(8,128)}) custom-call(bf16[128,2048]{1,0:T(8,128)(2,1)S(1)} %get-tuple-element.12.refs_0_, f32[512,512]{1,0:T(8,128)S(1)} %get-tuple-element.13.refs_1_, f32[512,512]{1,0:T(8,128)S(1)} %get-tuple-element.14.refs_2_, ...), custom_call_target="tpu_custom_call" | custom-call | tf_op jit(solution)/shard_map/finish/pallas_call | solution.py:480
